TPU v7x, 32 devices: a whole 2x2x4 slice. The times are simulated.
32 devices in a mesh: sp: 4 (over y, x), dp: 8 (over z, core).
Axes of the slice: x: 2, y: 2, z: 4, core: 2. Of those that a mesh axis runs over, the one named last changes fastest.
Arguments:
- value_half: bfloat16 [8, 1024, 2048], P('dp', 'sp'), may hold values from -6 to 6
- gate_half: bfloat16 [8, 1024, 2048], P('dp', 'sp'), may hold values from -6 to 6
- upstream: bfloat16 [8, 1024, 2048], P('dp', 'sp'), may hold values from -6 to 6
- conv_taps: float32 [31, 2048], P(None, 'sp'), may hold values from -1 to 1
- norm_gain: float32 [2048], replicated, may hold values from 0.1 to 1.9
- out_weight: bfloat16 [2048, 2048], P('dp'), may hold values from -0.125 to 0.125
Outputs:
- grad_value: bfloat16 [8, 1024, 2048], P('dp', 'sp')
- grad_gate: bfloat16 [8, 1024, 2048], P('dp', 'sp')
- grad_taps: float32 [31, 2048], P(None, 'sp')
- grad_gain: float32 [2048], replicated
- grad_weight: float32 [2048, 2048], P('dp')
All inputs are finite; a program needn't handle non-finite values.
Results may differ from a plain program's by a relative error of at most 0.0062.
Values may be sent and summed in bfloat16 or wider, within the bound.
A program may use at most 128 MiB of HBM per device.

v0:
```python
import jax
import jax.numpy as jnp
from jax import lax
from jax.sharding import PartitionSpec as P

NORM_EPS = 1e-05


def body(value_half, gate_half, upstream, conv_taps, norm_gain, out_weight):
    f32 = jnp.float32
    tap_count = conv_taps.shape[0]
    halo = tap_count - 1
    sp = lax.axis_size("sp")
    onward = [(i, i + 1) for i in range(sp - 1)]
    back = [(i + 1, i) for i in range(sp - 1)]
    value = value_half[0].astype(f32)
    gate = gate_half[0].astype(f32)
    length = value.shape[0]
    weight = lax.all_gather(out_weight, "dp", axis=0, tiled=True)
    up = upstream[0]
    up_columns = lax.all_to_all(up, "dp", split_axis=1, concat_axis=0, tiled=True)
    taps = lax.all_gather(conv_taps, "sp", axis=1, tiled=True)
    tail = (value[length - halo :] * jax.nn.sigmoid(gate[length - halo :])).astype(jnp.bfloat16)
    before = lax.ppermute(tail, "sp", onward)
    sig_gate = jax.nn.sigmoid(gate)
    glu = (value * sig_gate).astype(jnp.bfloat16)
    padded = jnp.concatenate([before, glu], axis=0).astype(f32)
    conv = jnp.zeros((length, padded.shape[1]), f32)
    for j in range(tap_count):
        conv = conv + taps[j] * padded[j : j + length]
    conv = conv.astype(jnp.bfloat16).astype(f32)
    mean = jnp.mean(conv, axis=-1, keepdims=True)
    centered = conv - mean
    inv = lax.rsqrt(jnp.mean(centered * centered, axis=-1, keepdims=True) + NORM_EPS)
    normed = centered * inv
    scaled = normed * norm_gain
    sig = jax.nn.sigmoid(scaled)
    activated = (scaled * sig).astype(jnp.bfloat16)
    act_all = lax.all_gather(activated, "dp", axis=0, tiled=True)
    grad_act = jnp.dot(up, weight, preferred_element_type=f32)
    grad_scaled = grad_act * sig * (1.0 + scaled * (1.0 - sig))
    gain_part = jnp.sum(grad_scaled * normed, axis=0)
    g = grad_scaled * norm_gain
    grad_conv = inv * (
        g
        - jnp.mean(g, axis=-1, keepdims=True)
        - normed * jnp.mean(g * normed, axis=-1, keepdims=True)
    )
    grad_conv = grad_conv.astype(jnp.bfloat16)
    after = lax.ppermute(grad_conv[:halo], "sp", back)
    extended = jnp.concatenate([grad_conv, after], axis=0).astype(f32)
    here = grad_conv.astype(f32)
    grad_glu = jnp.zeros_like(here)
    terms = []
    for j in range(tap_count):
        first = halo - j
        grad_glu = grad_glu + taps[j] * extended[first : first + length]
        terms.append(jnp.sum(here * padded[j : j + length], axis=0))
    sums = lax.psum(jnp.stack(terms + [gain_part]), ("sp", "dp"))
    width = conv_taps.shape[1]
    grad_taps = lax.dynamic_slice_in_dim(
        sums[:tap_count], lax.axis_index("sp") * width, width, axis=1
    )
    grad_gain = sums[tap_count]
    grad_glu = grad_glu.astype(jnp.bfloat16).astype(f32)
    grad_value = (grad_glu * sig_gate).astype(jnp.bfloat16)
    grad_gate = (grad_glu * value * sig_gate * (1.0 - sig_gate)).astype(jnp.bfloat16)
    owned = lax.dot_general(
        up_columns, act_all, (((0,), (0,)), ((), ())), preferred_element_type=f32
    )
    grad_weight = lax.psum(owned, "sp")
    return (grad_value[None], grad_gate[None], grad_taps, grad_gain, grad_weight)


def solution(mesh):
    tokens = P("dp", "sp", None)
    return jax.shard_map(
        body,
        mesh=mesh,
        in_specs=(tokens, tokens, tokens, P(None, "sp"), P(), P("dp", None)),
        out_specs=(tokens, tokens, P(None, "sp"), P(), P("dp", None)),
        check_vma=False,
    )
```

profile of v0, /device:TPU:0, one launch (start us, length us, event | category | flops | bytes accessed | tf_op | source)
XLA Modules:
  0.0 418.7 jit_solution(15272837373244284159)
XLA Ops:
  8.0 1.5 convert_element_type.49
  9.8 4.9 %collective-permute-start = (bf16[30,2048]{1,0:T(8,128)(2,1)S(1)}, bf16[30,2048]{1,0:T(8,128)(2,1)S(1)}, u32[]{:S(2)}, u32[]{:S(2)}) collective-permute-start(bf16[30,2048]{1,0:T(8,128)(2,1)S(1)} %fusion.96), channel_id=1, source_target_pairs={{0,8},{8,16},{16,24},{1,9},{9,17},{17,25},{2,10},{10,18},{18,26},{... | collective-permute-start | bytes 368648 | tf_op jit(solution)/shard_map/ppermute | solution.py:24
  14.7 9.1 %all_gather.9 = f32[31,2048]{1,0:T(8,128)S(1)} all-gather(f32[31,512]{1,0:T(8,128)S(1)} %copy-done.49), channel_id=1, replica_groups=mesh['sp'=4,'dp'=8] {'sp'}, dimensions={1}, use_global_device_ids=true | all-gather | bytes 317440 | tf_op jit(solution)/shard_map/all_gather | solution.py:22
  25.3 10.7 %convert_reduce_fusion = (f32[256]{0:T(256)S(1)}, bf16[256,2048]{1,0:T(8,128)(2,1)S(1)}) fusion(f32[286,2048]{1,0:T(8,128)S(1)} %maximum_convert_fusion, f32[2048]{0:T(1024)S(1)} %bitcast.106, f32[2048]{0:T(1024)S(1)} %bitcast.108, f32[2048]{0:T(1024)S(1)} %bitcast.110, f32[2048]{0:T(1024)S(1)} %bitcast.112, f32[2048]{0:T(1024)S(1)} %bitcast.114, ...), kind=kLoop, calls=%fused_computation.37 | loop fusion | flops 33554176 | bytes 66315264 | tf_op jit(solution)/shard_map/reduce_sum | solution.py:32
  37.6 56.8 %all-gather.3.cloned.1.call-done = bf16[2048,2048]{1,0:T(8,128)(2,1)} async-done(((bf16[256,2048]{1,0:T(8,128)(2,1)}), bf16[2048,2048]{1,0:T(8,128)(2,1)}) %all-gather.3.cloned.1.call-update) | async-done | bytes 8388624 | tf_op jit(solution)/shard_map/all_gather | solution.py:19
  94.4 9.5 %fusion.19 = (f32[2048]{0:T(1024)}, f32[256]{0:T(256)S(1)}, f32[256]{0:T(256)S(1)}, bf16[256,2048]{1,0:T(8,128)(2,1)}, f32[256,2048]{1,0:T(8,128)}) fusion(bf16[256,2048]{1,0:T(8,128)(2,1)} %copy-done.3, f32[256]{0:T(256)S(1)} %add_rsqrt_fusion, f32[256]{0:T(256)S(1)} %broadcast_multiply_fusion.2, f32[2048]{0:T(1024)} %param.10, ...), kind=kOutput, calls=%fused_computation.56 | convolution fusion | flops 2157966848 | bytes 13651968 | tf_op jit(solution)/shard_map/dot_general | solution.py:40
  103.9 2.3 copy.13
  106.2 4.4 %all-to-all-start = ((bf16[256,8,256]{0,2,1:T(8,128)(2,1)}), bf16[256,8,256]{0,2,1:T(8,128)(2,1)}, u32[]{:S(2)}, u32[]{:S(2)}) async-start(bf16[256,8,256]{0,2,1:T(8,128)(2,1)} %bitcast.102), calls=%async_computation | async-start | bytes 2097152 | tf_op jit(solution)/shard_map/all_to_all | solution.py:21
  110.7 54.7 %all-to-all-done = bf16[256,8,256]{0,2,1:T(8,128)(2,1)} async-done(((bf16[256,8,256]{0,2,1:T(8,128)(2,1)}), bf16[256,8,256]{0,2,1:T(8,128)(2,1)}, u32[]{:S(2)}, u32[]{:S(2)}) %all-to-all-start) | async-done | bytes 1048608 | tf_op jit(solution)/shard_map/all_to_all | solution.py:21
  165.4 2.3 copy.14
  167.7 8.2 %fusion.55 = (f32[2048]{0:T(1024)}, f32[2048]{0:T(1024)}, f32[2048]{0:T(1024)}, f32[2048]{0:T(1024)}, f32[2048]{0:T(1024)}, /*index=5*/f32[2048]{0:T(1024)}, f32...) fusion(f32[286,2048]{1,0:T(8,128)S(1)} %maximum_convert_fusion,, ...), kind=kLoop, calls=%fused_computation.92 | loop fusion | flops 24080384 | bytes 42102784 | tf_op jit(solution)/shard_map/reduce_sum | solution.py:58
  176.6 1.5 collective-permute-start.1
  178.1 4.2 %fusion.54 = (f32[2048]{0:T(1024)}, f32[2048]{0:T(1024)}, f32[2048]{0:T(1024)}, f32[2048]{0:T(1024)}, f32[2048]{0:T(1024)}, /*index=5*/f32[2048]{0:T(1024)}, f32...) fusion(bf16[256,2048]{1,0:T(8,128)(2,1)S(1)} %get-tuple-element, ...), kind=kLoop, calls=%fused_computation.91 | loop fusion | flops 14129152 | bytes 28418048 | tf_op jit(solution)/shard_map/reduce_sum | solution.py:58
  182.3 6.1 %stack.131 = f32[32,2048]{1,0:T(8,128)} concatenate(f32[1,2048]{1,0:T(1,128)} %bitcast.178, f32[1,2048]{1,0:T(1,128)} %bitcast.180, f32[1,2048]{1,0:T(1,128)} %bitcast.181, f32[1,2048]{1,0:T(1,128)} %bitcast.182, f32[1,2048]{1,0:T(1,128)} %bitcast.183, f32[1,2048]{1,0:T(1,128)} %bitcast.184, f32[1,2048]{1,0:T(1,128)} %bitcast.185, f32[1,2048]{1,0:T(1,128)} %bitcast.186, ...), dimensions={0} | concatenate | bytes 524288 | tf_op jit(solution)/shard_map/stack | solution.py:59
  188.5 1.5 maximum_convert_fusion.1
  190.0 16.3 %all-gather.5.cloned.1.call-done = bf16[2048,2048]{1,0:T(8,128)(2,1)} async-done(((bf16[256,2048]{1,0:T(8,128)(2,1)}), bf16[2048,2048]{1,0:T(8,128)(2,1)}) %all-gather.5.cloned.1.call-update) | async-done | bytes 8388624 | tf_op jit(solution)/shard_map/all_gather | solution.py:39
  206.4 7.4 %convolution_bitcast_fusion = f32[256,2048]{0,1:T(8,128)} fusion(bf16[2048,2048]{1,0:T(8,128)(2,1)} %all-gather.5.cloned.1.call-done, bf16[2048,256]{1,0:T(8,128)(2,1)} %bitcast.103), kind=kOutput, calls=%fused_computation.31 | convolution fusion | flops 2147483648 | bytes 11534336 | tf_op jit(solution)/shard_map/dot_general | solution.py:68
  214.7 10.6 %fusion.88 = (bf16[1,256,2048]{2,1,0:T(8,128)(2,1)}, bf16[256,2048]{1,0:T(8,128)(2,1)S(1)}) fusion(bf16[1,256,2048]{2,1,0:T(8,128)(2,1)} %param.6, bf16[1,256,2048]{2,1,0:T(8,128)(2,1)S(1)} %copy-done, f32[286,2048]{1,0:T(8,128)S(1)} %maximum_convert_fusion.1, f32[2048]{0:T(1024)S(1)} %bitcast.107, f32[2048]{0:T(1024)S(1)} %bitcast.109, ...), kind=kLoop, calls=%fused_computation.163 | loop fusion | flops 38273024 | bytes 69459968 | tf_op jit(solution)/shard_map/broadcast_in_dim | solution.py:72
  225.3 1.6 fusion.89
  226.8 110.4 %all-reduce.3.cloned.1.call-done = f32[32,2048]{1,0:T(8,128)} async-done(((f32[32,2048]{1,0:T(8,128)}), f32[32,2048]{1,0:T(8,128)}) %all-reduce.3.cloned.1.call-update) | async-done | bytes 262160 | tf_op jit(solution)/shard_map/psum | solution.py:59
  337.2 1.4 slice.556
  338.7 1.5 constant_dynamic-slice_fusion
  340.1 69.2 %all-reduce.5.cloned.1.call-done = f32[256,2048]{0,1:T(8,128)} async-done(((f32[256,2048]{0,1:T(8,128)}), f32[256,2048]{0,1:T(8,128)}) %all-reduce.5.cloned.1.call-update) | async-done | bytes 2097168 | tf_op jit(solution)/shard_map/psum | solution.py:71
  409.3 2.9 copy.15
  (123 shorter events, 5.3 us)
Async XLA Ops:
  7.2 2.3 copy-start
  7.2 87.2 %all-gather.3.cloned.1.call-start = ((), (), s32[]{:S(2)}) async-start(), calls=%async_computation.1 | async-start | bytes 9437184 | tf_op jit(solution)/shard_map/all_gather | solution.py:19
  7.9 198.4 %all-gather.5.cloned.1.call-start = ((), (), s32[]{:S(2)}) async-start(), calls=%async_computation.3 | async-start | bytes 9437184 | tf_op jit(solution)/shard_map/all_gather | solution.py:39
  9.4 5.3 %copy-start.49 = (f32[31,512]{1,0:T(8,128)S(1)}, f32[31,512]{1,0:T(8,128)}, u32[]{:S(2)}) copy-start(f32[31,512]{1,0:T(8,128)} %param.9) | copy-start | bytes 190468
  9.4 14.4 %copy-start.2 = (bf16[1,256,2048]{2,1,0:T(8,128)(2,1)S(1)}, bf16[1,256,2048]{2,1,0:T(8,128)(2,1)}, u32[]{:S(2)}) copy-start(bf16[1,256,2048]{2,1,0:T(8,128)(2,1)} %param.6) | copy-start | bytes 3145732
  9.8 15.0 %collective-permute-start = (bf16[30,2048]{1,0:T(8,128)(2,1)S(1)}, bf16[30,2048]{1,0:T(8,128)(2,1)S(1)}, u32[]{:S(2)}, u32[]{:S(2)}) collective-permute-start(bf16[30,2048]{1,0:T(8,128)(2,1)S(1)} %fusion.96), channel_id=1, source_target_pairs={{0,8},{8,16},{16,24},{1,9},{9,17},{17,25},{2,10},{10,18},{18,26},{... | collective-permute-start | bytes 368648 | tf_op jit(solution)/shard_map/ppermute | solution.py:24
  24.7 11.3 %copy-start.37 = (f32[1,2048]{1,0:T(1,128)}, f32[1,2048]{1,0:T(1,128)S(1)}, u32[]{:S(2)}) copy-start(f32[1,2048]{1,0:T(1,128)S(1)} %get-tuple-element.79) | copy-start | bytes 24580
  24.7 11.3 %copy-start.38 = (f32[1,2048]{1,0:T(1,128)}, f32[1,2048]{1,0:T(1,128)S(1)}, u32[]{:S(2)}) copy-start(f32[1,2048]{1,0:T(1,128)S(1)} %get-tuple-element.80) | copy-start | bytes 24580
  24.7 11.3 %copy-start.39 = (f32[1,2048]{1,0:T(1,128)}, f32[1,2048]{1,0:T(1,128)S(1)}, u32[]{:S(2)}) copy-start(f32[1,2048]{1,0:T(1,128)S(1)} %get-tuple-element.81) | copy-start | bytes 24580
  24.7 11.3 %copy-start.40 = (f32[1,2048]{1,0:T(1,128)}, f32[1,2048]{1,0:T(1,128)S(1)}, u32[]{:S(2)}) copy-start(f32[1,2048]{1,0:T(1,128)S(1)} %get-tuple-element.82) | copy-start | bytes 24580
  24.7 11.3 %copy-start.41 = (f32[1,2048]{1,0:T(1,128)}, f32[1,2048]{1,0:T(1,128)S(1)}, u32[]{:S(2)}) copy-start(f32[1,2048]{1,0:T(1,128)S(1)} %get-tuple-element.83) | copy-start | bytes 24580
  24.8 11.3 %copy-start.42 = (f32[1,2048]{1,0:T(1,128)}, f32[1,2048]{1,0:T(1,128)S(1)}, u32[]{:S(2)}) copy-start(f32[1,2048]{1,0:T(1,128)S(1)} %get-tuple-element.84) | copy-start | bytes 24580
  24.8 11.3 %copy-start.43 = (f32[1,2048]{1,0:T(1,128)}, f32[1,2048]{1,0:T(1,128)S(1)}, u32[]{:S(2)}) copy-start(f32[1,2048]{1,0:T(1,128)S(1)} %get-tuple-element.85) | copy-start | bytes 24580
  24.8 11.3 %copy-start.44 = (f32[1,2048]{1,0:T(1,128)}, f32[1,2048]{1,0:T(1,128)S(1)}, u32[]{:S(2)}) copy-start(f32[1,2048]{1,0:T(1,128)S(1)} %get-tuple-element.86) | copy-start | bytes 24580
  24.8 11.3 %copy-start.45 = (f32[1,2048]{1,0:T(1,128)}, f32[1,2048]{1,0:T(1,128)S(1)}, u32[]{:S(2)}) copy-start(f32[1,2048]{1,0:T(1,128)S(1)} %get-tuple-element.87) | copy-start | bytes 24580
  24.8 11.3 %copy-start.46 = (f32[1,2048]{1,0:T(1,128)}, f32[1,2048]{1,0:T(1,128)S(1)}, u32[]{:S(2)}) copy-start(f32[1,2048]{1,0:T(1,128)S(1)} %get-tuple-element.88) | copy-start | bytes 24580
  24.8 11.3 %copy-start.47 = (f32[1,2048]{1,0:T(1,128)}, f32[1,2048]{1,0:T(1,128)S(1)}, u32[]{:S(2)}) copy-start(f32[1,2048]{1,0:T(1,128)S(1)} %get-tuple-element.89) | copy-start | bytes 24580
  24.8 11.3 %copy-start.48 = (f32[1,2048]{1,0:T(1,128)}, f32[1,2048]{1,0:T(1,128)S(1)}, u32[]{:S(2)}) copy-start(f32[1,2048]{1,0:T(1,128)S(1)} %get-tuple-element.90) | copy-start | bytes 24580
  106.2 61.5 %copy-start.50 = (f32[2048]{0:T(1024)S(1)}, f32[2048]{0:T(1024)}, u32[]{:S(2)}) copy-start(f32[2048]{0:T(1024)} %param.10) | copy-start | bytes 24580
  106.2 59.1 %all-to-all-start = ((bf16[256,8,256]{0,2,1:T(8,128)(2,1)}), bf16[256,8,256]{0,2,1:T(8,128)(2,1)}, u32[]{:S(2)}, u32[]{:S(2)}) async-start(bf16[256,8,256]{0,2,1:T(8,128)(2,1)} %bitcast.102), calls=%async_computation | async-start | bytes 2097152 | tf_op jit(solution)/shard_map/all_to_all | solution.py:21
  110.6 226.6 %all-reduce.3.cloned.1.call-start = ((), (), s32[]{:S(2)}) async-start(), calls=%async_computation.2 | async-start | bytes 524288 | tf_op jit(solution)/shard_map/psum | solution.py:59
  175.9 6.4 %copy-start.1 = (bf16[256,2048]{1,0:T(8,128)(2,1)}, bf16[256,2048]{1,0:T(8,128)(2,1)S(1)}, u32[]{:S(2)}) copy-start(bf16[256,2048]{1,0:T(8,128)(2,1)S(1)} %get-tuple-element.54) | copy-start | bytes 3145732
  176.6 11.9 %collective-permute-start.1 = (bf16[30,2048]{1,0:T(8,128)(2,1)}, bf16[30,2048]{1,0:T(8,128)(2,1)S(1)}, u32[]{:S(2)}, u32[]{:S(2)}) collective-permute-start(bf16[30,2048]{1,0:T(8,128)(2,1)} %slice.523), channel_id=1, source_target_pairs={{8,0},{16,8},{24,16},{9,1},{17,9},{25,17},{10,2},{18,10},{26,18},{... | collective-permute-start | bytes 368648 | tf_op jit(solution)/shard_map/ppermute | solution.py:50
  188.5 220.8 %all-reduce.5.cloned.1.call-start = ((), (), s32[]{:S(2)}) async-start(), calls=%async_computation.4 | async-start | bytes 4194304 | tf_op jit(solution)/shard_map/psum | solution.py:71
  (34 other events, 34.7 us)
Sparse Core Ops, SparseCore 0:
  9.6 84.7 all-gather.2
  104.0 102.3 all-gather.4
  211.9 125.3 all-reduce.2
  340.8 68.5 all-reduce.4
where the time goes:
time: 419 us
  waiting for transfers between devices  308 us (74%)
  other arithmetic  39.9 us (10%)
  local copies, waits for them, and re-layouts  19.3 us (5%)
  matrix products  16.9 us (4%)
  between operations  14.5 us (3%)
  starting transfers between devices  10.9 us (3%)
  blocking collectives  9.08 us (2%)
    psum x1, waiting for transfers between devices, body(): sums = lax.psum(jnp.stack(terms + [gain_part]), ('sp', 'dp'))  110 us
    psum x1, waiting for transfers between devices, body(): grad_weight = lax.psum(owned, 'sp')  69.2 us
    all_gather x1, waiting for transfers between devices, body(): weight = lax.all_gather(out_weight, 'dp', axis=0, tiled=True)  56.8 us
    all_to_all x1, waiting for transfers between devices, body(): lax.all_to_all(up, 'dp', split_axis=1, concat_axis=0, tiled=True)  54.7 us
    all_gather x1, waiting for transfers between devices, body(): act_all = lax.all_gather(activated, 'dp', axis=0, tiled=True)  16.3 us
    reduce_sum x2, other arithmetic, body(): terms.append(jnp.sum(here * padded[j:j + length], axis=0))  12.5 us
    reduce_sum x1, other arithmetic, body(): mean = jnp.mean(conv, axis=-1, keepdims=True)  10.7 us
    broadcast_in_dim x1, other arithmetic, body(): grad_gate[None]  10.6 us
  transfers between devices with their start and end apart: 7, of which 5 were waited for; matrix products, arithmetic and copies ran while one was open for 15% of the time, Pallas kernels for 0%

commit v1 on v0

--- a/solution.py
+++ b/solution.py
@@ -4,6 +4,15 @@
 from jax.sharding import PartitionSpec as P
 
 NORM_EPS = 1e-05
+
+
+def _read_terms(array_in, axis_key):
+    n_chips = lax.psum(1, axis_key)
+    block_now = lambda h_now: [(j0, j0 ^ h_now) for j0 in range(n_chips)]
+    oldest = array_in
+    for to_i in range(n_chips.bit_length() - 1):
+        oldest = oldest + lax.ppermute(oldest, axis_key, block_now(1 << to_i))
+    return oldest
 
 
 def body(value_half, gate_half, upstream, conv_taps, norm_gain, out_weight):
@@ -68,7 +77,7 @@
     owned = lax.dot_general(
         up_columns, act_all, (((0,), (0,)), ((), ())), preferred_element_type=f32
     )
-    grad_weight = lax.psum(owned, "sp")
+    grad_weight = _read_terms(owned, "sp")
     return (grad_value[None], grad_gate[None], grad_taps, grad_gain, grad_weight)
 
 

time: 419 us -> 378 us (0.902)
  waiting for transfers between devices: 308 us -> 260 us
    psum x1 -> x0, waiting for transfers between devices: 69.2 us -> none  [body(): grad_weight = lax.psum(owned, 'sp')]
    psum x1, waiting for transfers between devices: 110 us -> 79.1 us  [body(): sums = lax.psum(jnp.stack(terms + [gain_part]), ('sp', 'dp'))]
    ppermute x1, waiting for transfers between devices: 0.01 us -> 30.4 us  [body(): after = lax.ppermute(grad_conv[:halo], 'sp', back)]
    all_gather x1, waiting for transfers between devices: 16.3 us -> 38.7 us  [body(): act_all = lax.all_gather(activated, 'dp', axis=0, tiled=True)]
    add x0 -> x2, other arithmetic: none -> 5.88 us  [_read_terms(): oldest = oldest + lax.ppermute(oldest, axis_key, block_now(1 << to_i))]
  transfers between devices with their start and end apart: 7 -> 8, of which waited for: 5 -> 5; matrix products, arithmetic and copies ran while one was open for 15% -> 15% of each run, Pallas kernels for 0% -> 0%
where the time goes in v1:
time: 378 us; the launch traced here: 377 us
  waiting for transfers between devices  260 us (69%)
  other arithmetic  43.6 us (12%)
  local copies, waits for them, and re-layouts  18.6 us (5%)
  matrix products  17.1 us (5%)
  between operations  14.8 us (4%)
  starting transfers between devices  13.7 us (4%)
  blocking collectives  9.08 us (2%)
    psum x1, waiting for transfers between devices, body(): sums = lax.psum(jnp.stack(terms + [gain_part]), ('sp', 'dp'))  79.1 us
    all_gather x1, waiting for transfers between devices, body(): weight = lax.all_gather(out_weight, 'dp', axis=0, tiled=True)  56.8 us
    all_to_all x1, waiting for transfers between devices, body(): lax.all_to_all(up, 'dp', split_axis=1, concat_axis=0, tiled=True)  54.5 us
    all_gather x1, waiting for transfers between devices, body(): act_all = lax.all_gather(activated, 'dp', axis=0, tiled=True)  38.7 us
    ppermute x1, waiting for transfers between devices, body(): after = lax.ppermute(grad_conv[:halo], 'sp', back)  30.4 us
    reduce_sum x2, other arithmetic, body(): terms.append(jnp.sum(here * padded[j:j + length], axis=0))  11.3 us
    reduce_sum x1, other arithmetic, body(): mean = jnp.mean(conv, axis=-1, keepdims=True)  10.7 us
    broadcast_in_dim x1, other arithmetic, body(): grad_gate[None]  9.5 us
  transfers between devices with their start and end apart: 8, of which 5 were waited for; matrix products, arithmetic and copies ran while one was open for 15% of the time, Pallas kernels for 0%

profile of v1, /device:TPU:0, one launch (start us, length us, event | category | flops | bytes accessed | tf_op | source)
XLA Modules:
  0.0 377.1 jit_solution(6353236624788869922)
XLA Ops:
  9.8 4.9 %collective-permute-start = (bf16[30,2048]{1,0:T(8,128)(2,1)S(1)}, bf16[30,2048]{1,0:T(8,128)(2,1)S(1)}, u32[]{:S(2)}, u32[]{:S(2)}) collective-permute-start(bf16[30,2048]{1,0:T(8,128)(2,1)S(1)} %fusion.96), channel_id=1, source_target_pairs={{0,8},{8,16},{16,24},{1,9},{9,17},{17,25},{2,10},{10,18},{18,26},{... | collective-permute-start | bytes 368648 | tf_op jit(solution)/shard_map/ppermute | solution.py:33
  14.7 9.1 %all_gather.9 = f32[31,2048]{1,0:T(8,128)S(1)} all-gather(f32[31,512]{1,0:T(8,128)S(1)} %copy-done.65), channel_id=1, replica_groups=mesh['sp'=4,'dp'=8] {'sp'}, dimensions={1}, use_global_device_ids=true | all-gather | bytes 317440 | tf_op jit(solution)/shard_map/all_gather | solution.py:31
  25.3 10.7 %convert_reduce_fusion = (f32[256]{0:T(256)S(1)}, bf16[256,2048]{1,0:T(8,128)(2,1)S(1)}) fusion(f32[286,2048]{1,0:T(8,128)S(1)} %maximum_convert_fusion, f32[2048]{0:T(1024)S(1)} %bitcast.106, f32[2048]{0:T(1024)S(1)} %bitcast.108, f32[2048]{0:T(1024)S(1)} %bitcast.110, f32[2048]{0:T(1024)S(1)} %bitcast.112, f32[2048]{0:T(1024)S(1)} %bitcast.114, ...), kind=kLoop, calls=%fused_computation.37 | loop fusion | flops 33554176 | bytes 66315264 | tf_op jit(solution)/shard_map/reduce_sum | solution.py:41
  37.6 56.8 %all-gather.3.cloned.1.call-done = bf16[2048,2048]{1,0:T(8,128)(2,1)} async-done(((bf16[256,2048]{1,0:T(8,128)(2,1)}), bf16[2048,2048]{1,0:T(8,128)(2,1)}) %all-gather.3.cloned.1.call-update) | async-done | bytes 8388624 | tf_op jit(solution)/shard_map/all_gather | solution.py:28
  94.4 9.5 %fusion.19 = (f32[2048]{0:T(1024)}, f32[256]{0:T(256)S(1)}, f32[256]{0:T(256)S(1)}, bf16[256,2048]{1,0:T(8,128)(2,1)}, f32[256,2048]{1,0:T(8,128)}) fusion(bf16[256,2048]{1,0:T(8,128)(2,1)} %copy-done.4, f32[256]{0:T(256)S(1)} %add_rsqrt_fusion, f32[256]{0:T(256)S(1)} %broadcast_multiply_fusion.2, f32[2048]{0:T(1024)} %param.10, ...), kind=kOutput, calls=%fused_computation.56 | convolution fusion | flops 2157966848 | bytes 13651968 | tf_op jit(solution)/shard_map/dot_general | solution.py:49
  103.9 2.3 copy.13
  106.1 4.3 %all-to-all-start = ((bf16[256,8,256]{0,2,1:T(8,128)(2,1)}), bf16[256,8,256]{0,2,1:T(8,128)(2,1)}, u32[]{:S(2)}, u32[]{:S(2)}) async-start(bf16[256,8,256]{0,2,1:T(8,128)(2,1)} %bitcast.102), calls=%async_computation | async-start | bytes 2097152 | tf_op jit(solution)/shard_map/all_to_all | solution.py:30
  110.6 54.5 %all-to-all-done = bf16[256,8,256]{0,2,1:T(8,128)(2,1)} async-done(((bf16[256,8,256]{0,2,1:T(8,128)(2,1)}), bf16[256,8,256]{0,2,1:T(8,128)(2,1)}, u32[]{:S(2)}, u32[]{:S(2)}) %all-to-all-start) | async-done | bytes 1048608 | tf_op jit(solution)/shard_map/all_to_all | solution.py:30
  165.2 2.3 copy.14
  167.4 38.7 %all-gather.5.cloned.1.call-done = bf16[2048,2048]{1,0:T(8,128)(2,1)} async-done(((bf16[256,2048]{1,0:T(8,128)(2,1)}), bf16[2048,2048]{1,0:T(8,128)(2,1)}) %all-gather.5.cloned.1.call-update) | async-done | bytes 8388624 | tf_op jit(solution)/shard_map/all_gather | solution.py:48
  206.2 7.6 %convolution_bitcast_fusion = f32[256,2048]{0,1:T(8,128)} fusion(bf16[2048,2048]{1,0:T(8,128)(2,1)} %all-gather.5.cloned.1.call-done, bf16[2048,256]{1,0:T(8,128)(2,1)} %bitcast.103), kind=kOutput, calls=%fused_computation.31 | convolution fusion | flops 2147483648 | bytes 11534336 | tf_op jit(solution)/shard_map/dot_general | solution.py:77
  215.3 7.1 %fusion.55 = (f32[2048]{0:T(1024)}, f32[2048]{0:T(1024)}, f32[2048]{0:T(1024)}, f32[2048]{0:T(1024)}, f32[2048]{0:T(1024)}, /*index=5*/f32[2048]{0:T(1024)}, f32...) fusion(f32[286,2048]{1,0:T(8,128)S(1)} %maximum_convert_fusion,, ...), kind=kLoop, calls=%fused_computation.92 | loop fusion | flops 24080384 | bytes 42102784 | tf_op jit(solution)/shard_map/reduce_sum | solution.py:67
  224.4 4.2 %fusion.54 = (f32[2048]{0:T(1024)}, f32[2048]{0:T(1024)}, f32[2048]{0:T(1024)}, f32[2048]{0:T(1024)}, f32[2048]{0:T(1024)}, /*index=5*/f32[2048]{0:T(1024)}, f32...) fusion(bf16[256,2048]{1,0:T(8,128)(2,1)S(1)} %get-tuple-element, ...), kind=kLoop, calls=%fused_computation.91 | loop fusion | flops 14129152 | bytes 28418048 | tf_op jit(solution)/shard_map/reduce_sum | solution.py:67
  228.6 6.1 %stack.131 = f32[32,2048]{1,0:T(8,128)} concatenate(f32[1,2048]{1,0:T(1,128)} %bitcast.178, f32[1,2048]{1,0:T(1,128)} %bitcast.180, f32[1,2048]{1,0:T(1,128)} %bitcast.181, f32[1,2048]{1,0:T(1,128)} %bitcast.182, f32[1,2048]{1,0:T(1,128)} %bitcast.183, f32[1,2048]{1,0:T(1,128)} %bitcast.184, f32[1,2048]{1,0:T(1,128)} %bitcast.185, f32[1,2048]{1,0:T(1,128)} %bitcast.186, ...), dimensions={0} | concatenate | bytes 524288 | tf_op jit(solution)/shard_map/stack | solution.py:68
  234.8 30.4 %collective-permute-done.1 = bf16[30,2048]{1,0:T(8,128)(2,1)S(1)} collective-permute-done((bf16[30,2048]{1,0:T(8,128)(2,1)}, bf16[30,2048]{1,0:T(8,128)(2,1)S(1)}, u32[]{:S(2)}, u32[]{:S(2)}) %collective-permute-start.1) | collective-permute-done | bytes 122912 | tf_op jit(solution)/shard_map/ppermute | solution.py:59
  265.1 1.5 maximum_convert_fusion.1
  266.9 2.7 add.289
  269.7 1.5 collective-permute-start.3
  271.5 9.5 %fusion.88 = (bf16[1,256,2048]{2,1,0:T(8,128)(2,1)}, bf16[256,2048]{1,0:T(8,128)(2,1)S(1)}) fusion(bf16[1,256,2048]{2,1,0:T(8,128)(2,1)S(1)} %copy-done.3, bf16[1,256,2048]{2,1,0:T(8,128)(2,1)S(1)} %copy-done, f32[286,2048]{1,0:T(8,128)S(1)} %maximum_convert_fusion.1, f32[2048]{0:T(1024)S(1)} %bitcast.107, f32[2048]{0:T(1024)S(1)} %bitcast.109, ...), kind=kLoop, calls=%fused_computation.163 | loop fusion | flops 38273024 | bytes 69459968 | tf_op jit(solution)/shard_map/broadcast_in_dim | solution.py:81
  281.0 1.6 fusion.89
  282.5 79.1 %all-reduce.2.cloned.1.call-done = f32[32,2048]{1,0:T(8,128)} async-done(((f32[32,2048]{1,0:T(8,128)}), f32[32,2048]{1,0:T(8,128)}) %all-reduce.2.cloned.1.call-update) | async-done | bytes 262160 | tf_op jit(solution)/shard_map/psum | solution.py:68
  363.0 1.5 constant_dynamic-slice_fusion
  364.5 3.2 add.290
  367.6 2.9 copy.15
  (158 shorter events, 10.4 us)
Async XLA Ops:
  7.2 87.2 %all-gather.3.cloned.1.call-start = ((), (), s32[]{:S(2)}) async-start(), calls=%async_computation.1 | async-start | bytes 9437184 | tf_op jit(solution)/shard_map/all_gather | solution.py:28
  7.9 198.3 %all-gather.5.cloned.1.call-start = ((), (), s32[]{:S(2)}) async-start(), calls=%async_computation.3 | async-start | bytes 9437184 | tf_op jit(solution)/shard_map/all_gather | solution.py:48
  9.4 14.4 %copy-start = (bf16[1,256,2048]{2,1,0:T(8,128)(2,1)S(1)}, bf16[1,256,2048]{2,1,0:T(8,128)(2,1)}, u32[]{:S(2)}) copy-start(bf16[1,256,2048]{2,1,0:T(8,128)(2,1)} %param.7) | copy-start | bytes 3145732
  9.8 15.0 %collective-permute-start = (bf16[30,2048]{1,0:T(8,128)(2,1)S(1)}, bf16[30,2048]{1,0:T(8,128)(2,1)S(1)}, u32[]{:S(2)}, u32[]{:S(2)}) collective-permute-start(bf16[30,2048]{1,0:T(8,128)(2,1)S(1)} %fusion.96), channel_id=1, source_target_pairs={{0,8},{8,16},{16,24},{1,9},{9,17},{17,25},{2,10},{10,18},{18,26},{... | collective-permute-start | bytes 368648 | tf_op jit(solution)/shard_map/ppermute | solution.py:33
  24.7 11.3 %copy-start.41 = (f32[1,2048]{1,0:T(1,128)}, f32[1,2048]{1,0:T(1,128)S(1)}, u32[]{:S(2)}) copy-start(f32[1,2048]{1,0:T(1,128)S(1)} %get-tuple-element.79) | copy-start | bytes 24580
  24.7 11.3 %copy-start.43 = (f32[1,2048]{1,0:T(1,128)}, f32[1,2048]{1,0:T(1,128)S(1)}, u32[]{:S(2)}) copy-start(f32[1,2048]{1,0:T(1,128)S(1)} %get-tuple-element.80) | copy-start | bytes 24580
  24.7 11.3 %copy-start.45 = (f32[1,2048]{1,0:T(1,128)}, f32[1,2048]{1,0:T(1,128)S(1)}, u32[]{:S(2)}) copy-start(f32[1,2048]{1,0:T(1,128)S(1)} %get-tuple-element.81) | copy-start | bytes 24580
  24.7 11.3 %copy-start.47 = (f32[1,2048]{1,0:T(1,128)}, f32[1,2048]{1,0:T(1,128)S(1)}, u32[]{:S(2)}) copy-start(f32[1,2048]{1,0:T(1,128)S(1)} %get-tuple-element.82) | copy-start | bytes 24580
  24.8 11.3 %copy-start.49 = (f32[1,2048]{1,0:T(1,128)}, f32[1,2048]{1,0:T(1,128)S(1)}, u32[]{:S(2)}) copy-start(f32[1,2048]{1,0:T(1,128)S(1)} %get-tuple-element.83) | copy-start | bytes 24580
  24.8 11.3 %copy-start.51 = (f32[1,2048]{1,0:T(1,128)}, f32[1,2048]{1,0:T(1,128)S(1)}, u32[]{:S(2)}) copy-start(f32[1,2048]{1,0:T(1,128)S(1)} %get-tuple-element.84) | copy-start | bytes 24580
  24.8 11.3 %copy-start.53 = (f32[1,2048]{1,0:T(1,128)}, f32[1,2048]{1,0:T(1,128)S(1)}, u32[]{:S(2)}) copy-start(f32[1,2048]{1,0:T(1,128)S(1)} %get-tuple-element.85) | copy-start | bytes 24580
  24.8 11.3 %copy-start.55 = (f32[1,2048]{1,0:T(1,128)}, f32[1,2048]{1,0:T(1,128)S(1)}, u32[]{:S(2)}) copy-start(f32[1,2048]{1,0:T(1,128)S(1)} %get-tuple-element.86) | copy-start | bytes 24580
  24.8 11.3 %copy-start.57 = (f32[1,2048]{1,0:T(1,128)}, f32[1,2048]{1,0:T(1,128)S(1)}, u32[]{:S(2)}) copy-start(f32[1,2048]{1,0:T(1,128)S(1)} %get-tuple-element.87) | copy-start | bytes 24580
  24.8 11.3 %copy-start.59 = (f32[1,2048]{1,0:T(1,128)}, f32[1,2048]{1,0:T(1,128)S(1)}, u32[]{:S(2)}) copy-start(f32[1,2048]{1,0:T(1,128)S(1)} %get-tuple-element.88) | copy-start | bytes 24580
  24.8 11.3 %copy-start.61 = (f32[1,2048]{1,0:T(1,128)}, f32[1,2048]{1,0:T(1,128)S(1)}, u32[]{:S(2)}) copy-start(f32[1,2048]{1,0:T(1,128)S(1)} %get-tuple-element.89) | copy-start | bytes 24580
  24.8 11.3 %copy-start.63 = (f32[1,2048]{1,0:T(1,128)}, f32[1,2048]{1,0:T(1,128)S(1)}, u32[]{:S(2)}) copy-start(f32[1,2048]{1,0:T(1,128)S(1)} %get-tuple-element.90) | copy-start | bytes 24580
  106.1 59.0 %all-to-all-start = ((bf16[256,8,256]{0,2,1:T(8,128)(2,1)}), bf16[256,8,256]{0,2,1:T(8,128)(2,1)}, u32[]{:S(2)}, u32[]{:S(2)}) async-start(bf16[256,8,256]{0,2,1:T(8,128)(2,1)} %bitcast.102), calls=%async_computation | async-start | bytes 2097152 | tf_op jit(solution)/shard_map/all_to_all | solution.py:30
  110.4 251.2 %all-reduce.2.cloned.1.call-start = ((), (), s32[]{:S(2)}) async-start(), calls=%async_computation.2 | async-start | bytes 524288 | tf_op jit(solution)/shard_map/psum | solution.py:68
  206.2 9.1 %copy-start.5 = (bf16[256,2048]{1,0:T(8,128)(2,1)S(1)}, bf16[256,2048]{1,0:T(8,128)(2,1)}, u32[]{:S(2)}) copy-start(bf16[256,2048]{1,0:T(8,128)(2,1)} %copy-done.4) | copy-start | bytes 3145732
  206.2 9.1 %copy-start.6 = (f32[256,2048]{1,0:T(8,128)S(1)}, f32[256,2048]{1,0:T(8,128)}, u32[]{:S(2)}) copy-start(f32[256,2048]{1,0:T(8,128)} %get-tuple-element.91) | copy-start | bytes 6291460
  206.2 9.1 %copy-start.66 = (f32[2048]{0:T(1024)S(1)}, f32[2048]{0:T(1024)}, u32[]{:S(2)}) copy-start(f32[2048]{0:T(1024)} %param.10) | copy-start | bytes 24580
  213.8 53.1 %collective-permute-start.2 = (f32[256,2048]{0,1:T(8,128)}, f32[256,2048]{0,1:T(8,128)}, u32[]{:S(2)}, u32[]{:S(2)}) collective-permute-start(f32[256,2048]{0,1:T(8,128)} %convolution_bitcast_fusion), channel_id=1, source_target_pairs={{0,8},{8,0},{16,24},{24,16},{1,9},{9,1},{17,25},{25,17},{2,10},{10... | collective-permute-start | bytes 6291464 | tf_op jit(solution)/shard_map/ppermute | solution.py:14
  223.1 42.0 %collective-permute-start.1 = (bf16[30,2048]{1,0:T(8,128)(2,1)}, bf16[30,2048]{1,0:T(8,128)(2,1)S(1)}, u32[]{:S(2)}, u32[]{:S(2)}) collective-permute-start(bf16[30,2048]{1,0:T(8,128)(2,1)} %slice.523), channel_id=1, source_target_pairs={{8,0},{16,8},{24,16},{9,1},{17,9},{25,17},{10,2},{18,10},{26,18},{... | collective-permute-start | bytes 368648 | tf_op jit(solution)/shard_map/ppermute | solution.py:59
  269.7 94.8 %collective-permute-start.3 = (f32[256,2048]{0,1:T(8,128)S(1)}, f32[256,2048]{0,1:T(8,128)}, u32[]{:S(2)}, u32[]{:S(2)}) collective-permute-start(f32[256,2048]{0,1:T(8,128)S(1)} %add.289), channel_id=1, source_target_pairs={{0,16},{8,24},{16,0},{24,8},{1,17},{9,25},{17,1},{25,9},{2,18},{10... | collective-permute-start | bytes 6291464 | tf_op jit(solution)/shard_map/ppermute | solution.py:14
  (51 other events, 172.4 us)
Sparse Core Ops, SparseCore 0:
  9.6 84.7 all-gather.2
  104.0 102.1 all-gather.4
  234.9 126.6 all-reduce.1
